TPU v7x, 32 devices: a whole 2x2x4 slice. The times are simulated.
32 devices in a mesh: gr: 2 (over x), sp: 8 (over z, y), tp: 2 (over core).
Axes of the slice: x: 2, y: 2, z: 4, core: 2. Of those that a mesh axis runs over, the one named last changes fastest.
Arguments:
- tokens: bfloat16 [8, 2048, 2048], P('gr', 'sp'), parts along dimension 0, may hold values from -6 to 6
- new_rows: bfloat16 [8, 2048], P('gr'), parts along dimension 0, may hold values from -6 to 6
- new_query: bfloat16 [8, 1024], P('gr', 'tp'), parts along dimension 0, may hold values from -6 to 6
- norm_gain: bfloat16 [2048], replicated, may hold values from 0.099609375 to 1.8984375
- key_weight: bfloat16 [2048, 1024], P('sp', 'tp'), may hold values from -0.125 to 0.125
- value_weight: bfloat16 [2048, 2048], P('sp', 'tp'), may hold values from -0.125 to 0.125
- input_weight: bfloat16 [2048, 16], replicated, may hold values from -0.125 to 0.125
- forget_weight: bfloat16 [2048, 16], replicated, may hold values from -0.125 to 0.125
- forget_bias: float32 [16], P('tp'), may hold values from 3 to 12
- gate_offsets: float32 [8, 2048, 2, 16], P('gr', 'sp', None, 'tp'), parts along dimension 0, may hold values from -6 to 250, as said below
Outputs:
- cache_keys: bfloat16 [16, 1024, 1024], P(('gr', 'sp'), None, 'tp'), parts along dimension 0
- cache_values: bfloat16 [16, 1024, 2048], P(('gr', 'sp'), None, 'tp'), parts along dimension 0
- cache_weights: float32 [16, 16, 1024], P(('gr', 'sp'), 'tp'), parts along dimension 0
- first_read: bfloat16 [8, 2048], P('gr', 'tp'), parts along dimension 0
There are 2 independent parts, one for each index of `gr`. A program takes and returns all parts, laid end to end along the dimension named above; an argument that names none is the same for every part. Nothing has to cross between parts.
Inputs may be any that keep to these rules, and one draw needn't show every extreme that they name: `gate_offsets`: entry 1 along the third dimension is never positive.
All inputs are finite; a program needn't handle non-finite values.
Results may differ from a plain program's by a relative error of at most 0.012.
The roundings to bfloat16 on the way count: a program that leaves them out, or rounds other values in their place, can miss the bound.
Values may be sent and summed in bfloat16 or wider, within the bound.
A program may use at most 64 MiB of HBM per device.

v0:
```python
import jax
import jax.numpy as jnp
from jax import lax
from jax.sharding import PartitionSpec as P

EPSILON = 1e-06
HIGHEST = lax.Precision.HIGHEST


def normed_rows(source, norm_gain):
    widened = source.astype(jnp.float32)
    inverse_rms = lax.rsqrt(jnp.mean(widened * widened, axis=-1, keepdims=True) + EPSILON)
    return (widened * inverse_rms * norm_gain.astype(jnp.float32)).astype(jnp.bfloat16)


def contract_last(a, b):
    return lax.dot_general(a, b, (((1,), (1,)), ((), ())), preferred_element_type=jnp.float32)


def log_weights(gates, offsets, forget_bias, heads, blocks, pieces):
    rows = gates.shape[1]
    sub = rows // blocks
    input_gate = gates[:heads] + offsets[:heads]
    log_forget = jax.nn.log_sigmoid(gates[heads:] + forget_bias[:, None]) + offsets[heads:]
    by_block = log_forget.reshape(heads, blocks, sub)
    later = jnp.tril(jnp.ones((sub, sub), jnp.float32), -1)
    within = jnp.dot(by_block.reshape(heads * blocks, sub), later, precision=HIGHEST)
    totals = jnp.sum(by_block, axis=2)
    index = lax.axis_index("sp")
    everything = lax.all_gather(totals, "sp")
    ours = lax.dynamic_slice_in_dim(everything, index // pieces * pieces, pieces, 0)
    piece = index % pieces
    all_pieces = jnp.sum(ours, axis=0)
    after = jnp.flip(jnp.cumsum(jnp.flip(all_pieces, 1), axis=1), 1) - all_pieces
    follows = (jnp.arange(pieces) > piece).astype(jnp.float32)
    after = after + jnp.sum(ours * follows[:, None, None], axis=0)
    suffix = within.reshape(heads, blocks, sub) + after[:, :, None]
    return input_gate + suffix.reshape(heads, rows)


def read_part(query, keys, values, log_weight, heads):
    key_size = keys.shape[1] // heads
    value_size = values.shape[1] // heads
    peak = jnp.max(log_weight, axis=1, keepdims=True)
    own_head = jnp.arange(heads)[:, None] == jnp.arange(keys.shape[1])[None, :] // key_size
    spread = jnp.where(own_head, query, jnp.zeros_like(query))
    scores = contract_last(spread, keys)
    terms = jnp.exp(log_weight - peak) * scores
    wide = jnp.dot(terms.astype(jnp.bfloat16), values, preferred_element_type=jnp.float32)
    pick = jnp.eye(heads, dtype=jnp.float32)
    numerator = jnp.sum(wide.reshape(heads, heads, value_size) * pick[:, :, None], axis=1)
    return (peak, numerator, jnp.sum(terms, axis=1, keepdims=True))


def finish(peak, numerator, denominator, own_score, gate_new, value_new, seq_count, pieces):
    heads, value_size = numerator.shape
    one = jnp.concatenate([peak, denominator, own_score, gate_new], axis=1)
    one = jnp.pad(one, ((0, 0), (0, value_size - one.shape[1])))
    packed = jnp.concatenate([numerator, value_new, one], axis=1)
    everything = lax.all_gather(packed, "sp").reshape(seq_count, pieces, heads, -1)
    one = everything[..., 2 * value_size :]
    peaks, denominators = (one[..., 0], one[..., 1])
    own_score, gate_new = (one[:, 0, :, 2], one[:, 0, :, 3])
    value_new = everything[:, 0, :, value_size : 2 * value_size]
    top = jnp.maximum(jnp.max(peaks, axis=1), gate_new)
    old = jnp.exp(peaks - top[:, None])
    new = jnp.exp(gate_new - top) * own_score
    total = jnp.sum(old[..., None] * everything[..., :value_size], axis=1)
    total = total + new[..., None] * value_new
    weight = jnp.sum(old * denominators, axis=1) + new
    return total / jnp.maximum(jnp.abs(weight), 1.0)[..., None]


def per_device(
    tokens,
    new_rows,
    new_query,
    norm_gain,
    key_weight,
    value_weight,
    input_weight,
    forget_weight,
    forget_bias,
    gate_offsets,
):
    seq_count, positions, model_width = tokens.shape
    heads = forget_bias.shape[0]
    key_size = key_weight.shape[1] // heads
    group = lax.axis_size("sp")
    shares = lax.axis_size("tp")
    pieces = group // seq_count
    sub = positions // pieces
    rows = group * sub
    index, core = (lax.axis_index("sp"), lax.axis_index("tp"))
    prompt = index // pieces
    part = model_width // shares
    mine = lax.dynamic_slice_in_dim(tokens.reshape(group, sub, model_width), core * part, part, 2)
    moved = lax.all_to_all(mine, "sp", split_axis=0, concat_axis=0, tiled=True)
    source = lax.all_gather(moved.reshape(rows, part), "tp", axis=1, tiled=True)
    offsets = jnp.transpose(gate_offsets.reshape(group, sub, 2 * heads), (0, 2, 1))
    offsets = lax.all_to_all(offsets, "sp", split_axis=0, concat_axis=0, tiled=True)
    offsets = jnp.transpose(offsets, (1, 0, 2)).reshape(2 * heads, rows)
    key_weight = lax.all_gather(key_weight, "sp", axis=0, tiled=True)
    value_weight = lax.all_gather(value_weight, "sp", axis=0, tiled=True)
    normed = normed_rows(source, norm_gain)
    fresh = normed_rows(lax.dynamic_slice_in_dim(new_rows, prompt, 1, 0), norm_gain)
    head_start = core * heads
    gate_weight = jnp.concatenate(
        [
            lax.dynamic_slice_in_dim(input_weight, head_start, heads, 1),
            lax.dynamic_slice_in_dim(forget_weight, head_start, heads, 1),
        ],
        axis=1,
    ).T
    gates = contract_last(gate_weight, normed)
    gate_new = contract_last(gate_weight[:heads], fresh)

    def project(x):
        keys = jnp.dot(x, key_weight, preferred_element_type=jnp.float32) * key_size ** (-0.5)
        values = jnp.dot(x, value_weight, preferred_element_type=jnp.float32)
        return (keys.astype(jnp.bfloat16), values.astype(jnp.bfloat16))

    keys, values = project(normed)
    key_new, value_new = project(fresh)
    log_weight = log_weights(gates, offsets, forget_bias, heads, group, pieces)
    query = lax.dynamic_slice_in_dim(new_query, prompt, 1, 0)
    peak, numerator, denominator = read_part(query, keys, values, log_weight, heads)
    own_score = jnp.sum(
        (query.astype(jnp.float32) * key_new.astype(jnp.float32)).reshape(heads, key_size),
        axis=1,
        keepdims=True,
    )
    value_new = value_new.astype(jnp.float32).reshape(heads, -1)
    read_out = finish(
        peak, numerator, denominator, own_score, gate_new, value_new, seq_count, pieces
    )
    return (
        keys[None],
        values[None],
        log_weight[None],
        read_out.reshape(seq_count, -1).astype(jnp.bfloat16),
    )


def solution(mesh):
    return jax.shard_map(
        per_device,
        mesh=mesh,
        in_specs=(
            P("gr", "sp", None),
            P("gr", None),
            P("gr", "tp"),
            P(),
            P("sp", "tp"),
            P("sp", "tp"),
            P(),
            P(),
            P("tp"),
            P("gr", "sp", None, "tp"),
        ),
        out_specs=(
            P(("gr", "sp"), None, "tp"),
            P(("gr", "sp"), None, "tp"),
            P(("gr", "sp"), "tp", None),
            P("gr", "tp"),
        ),
        check_vma=False,
    )
```

profile of v0, /device:TPU:0, one launch (start us, length us, event | category | flops | bytes accessed | tf_op | source)
XLA Modules:
  0.0 263.4 jit_solution(13032726843708910737)
XLA Ops:
  7.2 0.7 all-gather.8.cloned.1.call-update
  7.9 0.7 all-gather.10.cloned.1.call-update
  8.7 1.8 constant_dynamic-slice_fusion.4
  10.5 80.9 %all_to_all.10 = bf16[8,128,1024]{2,1,0:T(8,128)(2,1)} all-to-all(bf16[8,128,1024]{2,1,0:T(8,128)(2,1)S(1)} %constant_dynamic-slice_fusion.4), channel_id=1, replica_groups=mesh['gr'=2,'sp'=8,'tp'=2] {'sp'}, dimensions={0} | all-to-all | bytes 4194304 | tf_op jit(solution)/shard_map/all_to_all | solution.py:98
  91.5 0.6 copy.36
  92.2 3.6 %all-to-all-start.1 = ((f32[8,16,128]{2,1,0:T(8,128)}), f32[8,16,128]{2,1,0:T(8,128)S(1)}, u32[]{:S(2)}, u32[]{:S(2)}) async-start(f32[8,16,128]{2,1,0:T(8,128)} %copy.36), calls=%async_computation.1 | async-start | bytes 131072 | tf_op jit(solution)/shard_map/all_to_all | solution.py:101
  95.8 0.6 multiply_reduce_fusion
  97.4 2.0 fusion.27
  99.7 61.1 %all-gather.10.cloned.1.call-done = bf16[2048,1024]{1,0:T(8,128)(2,1)} async-done(((bf16[256,1024]{1,0:T(8,128)(2,1)}), bf16[2048,1024]{1,0:T(8,128)(2,1)}) %all-gather.10.cloned.1.call-update) | async-done | bytes 4194320 | tf_op jit(solution)/shard_map/all_gather | solution.py:104
  160.8 2.8 %fusion.29 = f32[1,1024]{1,0:T(1,128)S(1)} fusion(bf16[2048,1024]{1,0:T(8,128)(2,1)} %all-gather.10.cloned.1.call-done, bf16[1,2048]{1,0:T(2,128)(2,1)S(1)} %multiply_multiply_fusion), kind=kOutput, calls=%fused_computation.55 | convolution fusion | flops 4194304 | bytes 4202496 | tf_op jit(solution)/shard_map/dot_general | solution.py:120
  163.6 10.9 %all-gather.6.cloned.1.call-done = bf16[1024,2048]{1,0:T(8,128)(2,1)} async-done(((bf16[1024,1024]{1,0:T(8,128)(2,1)}), bf16[1024,2048]{1,0:T(8,128)(2,1)}) %all-gather.6.cloned.1.call-update) | async-done | bytes 4194320 | tf_op jit(solution)/shard_map/all_gather | solution.py:99
  174.6 3.2 %fusion = f32[1024]{0:T(1024)S(1)} fusion(bf16[1024,2048]{1,0:T(8,128)(2,1)} %all-gather.6.cloned.1.call-done), kind=kLoop, calls=%fused_computation.2 | loop fusion | flops 6290432 | bytes 4198400 | tf_op jit(solution)/shard_map/reduce_sum | solution.py:12
  177.8 0.2 copy-done
  178.0 1.3 fusion.9
  179.3 0.2 fusion.52
  179.5 30.9 %all-gather = f32[64,8]{1,0:T(8,128)S(1)} all-gather(f32[8,8]{1,0:T(8,128)S(1)} %copy.38), channel_id=2, replica_groups=mesh['gr'=2,'sp'=8,'tp'=2] {'sp'}, dimensions={0}, use_global_device_ids=true | all-gather | bytes 2304 | tf_op jit(solution)/shard_map/all_gather | solution.py:30
  210.9 0.3 fusion.4
  211.3 4.6 %multiply_convert_fusion = bf16[1024,512]{1,0:T(8,128)(2,1)S(1)} fusion(bf16[2048,512]{1,0:T(8,128)(2,1)S(1)} %copy-done.1, bf16[1024,2048]{1,0:T(8,128)(2,1)} %all-gather.6.cloned.1.call-done, f32[2048]{0:T(1024)S(1)} %convert_element_type.64, f32[1024]{0:T(1024)S(1)} %add_rsqrt_fusion), kind=kOutput, calls=%fused_computation.5 | convolution fusion | flops 2156920832 | bytes 7352320 | tf_op jit(solution)/shard_map/dot_general | solution.py:119
  215.9 0.5 fusion.54
  216.5 8.0 %convolution_convert_fusion = bf16[1024,1024]{1,0:T(8,128)(2,1)S(1)} fusion(bf16[2048,1024]{1,0:T(8,128)(2,1)} %all-gather.10.cloned.1.call-done, bf16[1024,2048]{1,0:T(8,128)(2,1)} %all-gather.6.cloned.1.call-done, f32[2048]{0:T(1024)S(1)} %convert_element_type.64, f32[1024]{0:T(1024)S(1)} %add_rsqrt_fusion), kind=kOutput, calls=%fused_computation.6 | convolution fusion | flops 4304404480 | bytes 10498048 | tf_op jit(solution)/shard_map/dot_general | solution.py:120
  224.6 0.4 fusion.5
  225.0 30.5 %all-gather.1 = f32[64,384]{1,0:T(8,128)S(1)} all-gather(f32[8,384]{1,0:T(8,128)S(1)} %pad_maximum_fusion.2), channel_id=3, replica_groups=mesh['gr'=2,'sp'=8,'tp'=2] {'sp'}, dimensions={0}, use_global_device_ids=true | all-gather | bytes 110592 | tf_op jit(solution)/shard_map/all_gather | solution.py:60
  255.8 0.2 exponential_reduce_fusion
  256.3 0.6 fusion.24
  (72 shorter events, 2.1 us)
Async XLA Ops:
  7.2 90.2 %all-gather.8.cloned.1.call-start = ((), (), s32[]{:S(2)}) async-start(), calls=%async_computation.3 | async-start | bytes 2359296 | tf_op jit(solution)/shard_map/all_gather | solution.py:103
  7.9 152.9 %all-gather.10.cloned.1.call-start = ((), (), s32[]{:S(2)}) async-start(), calls=%async_computation.4 | async-start | bytes 4718592 | tf_op jit(solution)/shard_map/all_gather | solution.py:104
  8.6 165.9 %all-gather.6.cloned.1.call-start = ((), (), s32[]{:S(2)}) async-start(), calls=%async_computation.2 | async-start | bytes 6291456 | tf_op jit(solution)/shard_map/all_gather | solution.py:99
  10.5 81.0 %copy-start.5 = (f32[4,256,2,8]{1,3,2,0:T(8,128)S(1)}, f32[4,256,2,8]{1,3,2,0:T(8,128)}, u32[]{:S(2)}) copy-start(f32[4,256,2,8]{1,3,2,0:T(8,128)} %param.19) | copy-start | bytes 196612
  10.5 85.3 %copy-start.6 = (bf16[4,2048]{1,0:T(4,128)(2,1)S(1)}, bf16[4,2048]{1,0:T(4,128)(2,1)}, u32[]{:S(2)}) copy-start(bf16[4,2048]{1,0:T(4,128)(2,1)} %param.11) | copy-start | bytes 49156
  10.5 86.6 %copy-start.9 = (bf16[2048]{0:T(1024)(128)(2,1)S(1)}, bf16[2048]{0:T(1024)(128)(2,1)}, u32[]{:S(2)}) copy-start(bf16[2048]{0:T(1024)(128)(2,1)} %param.13) | copy-start | bytes 12292
  10.5 86.6 %copy-start.10 = (bf16[4,512]{1,0:T(4,128)(2,1)S(1)}, bf16[4,512]{1,0:T(4,128)(2,1)}, u32[]{:S(2)}) copy-start(bf16[4,512]{1,0:T(4,128)(2,1)} %param.12) | copy-start | bytes 12292
  10.5 86.7 %copy-start.7 = (bf16[2048,16]{0,1:T(8,128)(2,1)S(1)}, bf16[2048,16]{0,1:T(8,128)(2,1)}, u32[]{:S(2)}) copy-start(bf16[2048,16]{0,1:T(8,128)(2,1)} %param.17) | copy-start | bytes 196612
  10.5 86.7 %copy-start.8 = (bf16[2048,16]{0,1:T(8,128)(2,1)S(1)}, bf16[2048,16]{0,1:T(8,128)(2,1)}, u32[]{:S(2)}) copy-start(bf16[2048,16]{0,1:T(8,128)(2,1)} %param.16) | copy-start | bytes 196612
  92.2 87.1 %all-to-all-start.1 = ((f32[8,16,128]{2,1,0:T(8,128)}), f32[8,16,128]{2,1,0:T(8,128)S(1)}, u32[]{:S(2)}, u32[]{:S(2)}) async-start(f32[8,16,128]{2,1,0:T(8,128)} %copy.36), calls=%async_computation.1 | async-start | bytes 131072 | tf_op jit(solution)/shard_map/all_to_all | solution.py:101
  174.6 3.4 %copy-start = (bf16[1024,2048]{1,0:T(8,128)(2,1)S(1)}, bf16[1024,2048]{1,0:T(8,128)(2,1)}, u32[]{:S(2)}) copy-start(bf16[1024,2048]{1,0:T(8,128)(2,1)} %all-gather.6.cloned.1.call-done) | copy-start | bytes 12582916
  177.8 1.5 copy-start.11
  178.0 33.3 %copy-start.1 = (bf16[2048,512]{1,0:T(8,128)(2,1)S(1)}, bf16[2048,512]{1,0:T(8,128)(2,1)}, u32[]{:S(2)}) copy-start(bf16[2048,512]{1,0:T(8,128)(2,1)} %all-gather.8.cloned.1.call-done) | copy-start | bytes 6291460
  211.3 4.7 %copy-start.4 = (f32[8,1024]{1,0:T(8,128)}, f32[8,1024]{1,0:T(8,128)S(1)}, u32[]{:S(2)}) copy-start(f32[8,1024]{1,0:T(8,128)S(1)} %get-tuple-element.12) | copy-start | bytes 98308
  215.9 8.6 %copy-start.3 = (bf16[1024,512]{1,0:T(8,128)(2,1)}, bf16[1024,512]{1,0:T(8,128)(2,1)S(1)}, u32[]{:S(2)}) copy-start(bf16[1024,512]{1,0:T(8,128)(2,1)S(1)} %multiply_convert_fusion) | copy-start | bytes 3145732
  224.5 32.4 %copy-start.2 = (bf16[1024,1024]{1,0:T(8,128)(2,1)}, bf16[1024,1024]{1,0:T(8,128)(2,1)S(1)}, u32[]{:S(2)}) copy-start(bf16[1024,1024]{1,0:T(8,128)(2,1)S(1)} %convolution_convert_fusion) | copy-start | bytes 6291460
Sparse Core Ops, SparseCore 0:
  10.1 76.4 all-gather.7
  88.7 72.0 all-gather.9
  162.3 12.1 all-gather.5
where the time goes:
time: 264 us; the launch traced here: 263 us
  blocking collectives  142 us (54%)
  waiting for transfers between devices  73.4 us (28%)
  matrix products  19.9 us (8%)
  between operations  14.8 us (6%)
  other arithmetic  5.59 us (2%)
  local copies, waits for them, and re-layouts  3.73 us (1%)
  starting transfers between devices  3.71 us (1%)
    all_to_all x1, blocking collectives, per_device(): moved = lax.all_to_all(mine, 'sp', split_axis=0, concat_axis=0, tiled=True)  80.9 us
    all_gather x1, waiting for transfers between devices, per_device(): value_weight = lax.all_gather(value_weight, 'sp', axis=0, tiled=True)  61.1 us
    all_gather x1, blocking collectives, log_weights(): everything = lax.all_gather(totals, 'sp')  30.9 us
    all_gather x1, blocking collectives, finish(): lax.all_gather(packed, 'sp').reshape(seq_count, pieces, heads, -1)  30.5 us
    all_gather x1, waiting for transfers between devices, per_device(): source = lax.all_gather(moved.reshape(rows, part), 'tp', axis=1, tiled=True)  10.9 us
    dot_general x2, matrix products, project(): values = jnp.dot(x, value_weight, preferred_element_type=jnp.float32)  10.8 us
    dot_general x2, matrix products, project(): jnp.dot(x, key_weight, preferred_element_type=jnp.float32)  6.53 us
  transfers between devices with their start and end apart: 4, of which 2 were waited for; matrix products, arithmetic and copies ran while one was open for 5% of the time, Pallas kernels for 0%

commit v1 on v0

--- a/solution.py
+++ b/solution.py
@@ -101,7 +101,12 @@
     offsets = lax.all_to_all(offsets, "sp", split_axis=0, concat_axis=0, tiled=True)
     offsets = jnp.transpose(offsets, (1, 0, 2)).reshape(2 * heads, rows)
     key_weight = lax.all_gather(key_weight, "sp", axis=0, tiled=True)
-    value_weight = lax.all_gather(value_weight, "sp", axis=0, tiled=True)
+    ring = [value_weight]
+    for hop in range(7):
+        ring.append(lax.ppermute(ring[-1], "sp", [(dev, (dev + 1) % 8) for dev in range(8)]))
+    value_weight = jnp.roll(
+        jnp.concatenate(ring[::-1], axis=0), (lax.axis_index("sp") + 1) * ring[0].shape[0], axis=0
+    )
     normed = normed_rows(source, norm_gain)
     fresh = normed_rows(lax.dynamic_slice_in_dim(new_rows, prompt, 1, 0), norm_gain)
     head_start = core * heads

time: 264 us -> 287 us (1.087)
  blocking collectives: 142 us -> 61.1 us
  waiting for transfers between devices: 73.4 us -> 139 us
  starting transfers between devices: 3.71 us -> 30.7 us
  local copies, waits for them, and re-layouts: 3.73 us -> 14.7 us
    ppermute x0 -> x7, waiting for transfers between devices: none -> 138 us  [per_device(): lax.ppermute(ring[-1], 'sp', [(dev, (dev + 1) % 8) for dev in range(8)])]
    all_to_all x1 -> x0, blocking collectives: 80.9 us -> none  [per_device(): moved = lax.all_to_all(mine, 'sp', split_axis=0, concat_axis=0, tiled=True)]
    all_gather x1 -> x0, waiting for transfers between devices: 61.1 us -> none  [per_device(): value_weight = lax.all_gather(value_weight, 'sp', axis=0, tiled=True)]
    all_gather x1, waiting for transfers between devices: 10.9 us -> 0.01 us  [per_device(): source = lax.all_gather(moved.reshape(rows, part), 'tp', axis=1, tiled=True)]
    all_to_all x1, starting transfers between devices: 3.59 us -> 13.6 us  [per_device(): lax.all_to_all(offsets, 'sp', split_axis=0, concat_axis=0, tiled=True)]
    ppermute x0 -> x7, starting transfers between devices: none -> 9.76 us  [per_device(): lax.ppermute(ring[-1], 'sp', [(dev, (dev + 1) % 8) for dev in range(8)])]
    unnamed x30 -> x53, local copies, waits for them, and re-layouts: 0.6 us -> 10.2 us
    all_to_all x0 -> x1, starting transfers between devices: none -> 7.31 us  [per_device(): moved = lax.all_to_all(mine, 'sp', split_axis=0, concat_axis=0, tiled=True)]
  transfers between devices with their start and end apart: 4 -> 11, of which waited for: 2 -> 6; matrix products, arithmetic and copies ran while one was open for 5% -> 6% of each run, Pallas kernels for 0% -> 0%
where the time goes in v1:
time: 287 us
  waiting for transfers between devices  139 us (48%)
  blocking collectives  61.1 us (21%)
  starting transfers between devices  30.7 us (11%)
  matrix products  19.9 us (7%)
  between operations  15.2 us (5%)
  local copies, waits for them, and re-layouts  14.7 us (5%)
  other arithmetic  5.44 us (2%)
    ppermute x7, waiting for transfers between devices, per_device(): lax.ppermute(ring[-1], 'sp', [(dev, (dev + 1) % 8) for dev in range(8)])  138 us
    all_gather x1, blocking collectives, log_weights(): everything = lax.all_gather(totals, 'sp')  30.6 us
    all_gather x1, blocking collectives, finish(): lax.all_gather(packed, 'sp').reshape(seq_count, pieces, heads, -1)  30.5 us
    all_to_all x1, starting transfers between devices, per_device(): lax.all_to_all(offsets, 'sp', split_axis=0, concat_axis=0, tiled=True)  13.6 us
    unnamed x53, local copies, waits for them, and re-layouts  10.2 us
    ppermute x7, starting transfers between devices, per_device(): lax.ppermute(ring[-1], 'sp', [(dev, (dev + 1) % 8) for dev in range(8)])  9.76 us
    dot_general x2, matrix products, project(): values = jnp.dot(x, value_weight, preferred_element_type=jnp.float32)  8.65 us
    all_to_all x1, starting transfers between devices, per_device(): moved = lax.all_to_all(mine, 'sp', split_axis=0, concat_axis=0, tiled=True)  7.31 us
  transfers between devices with their start and end apart: 11, of which 6 were waited for; matrix products, arithmetic and copies ran while one was open for 6% of the time, Pallas kernels for 0%

profile of v1, /device:TPU:0, one launch (start us, length us, event | category | flops | bytes accessed | tf_op | source)
XLA Modules:
  0.0 286.6 jit_solution(12414046209437848840)
XLA Ops:
  7.2 3.1 %constant_dynamic-slice_fusion.4 = bf16[8,128,1024]{2,1,0:T(8,128)(2,1)} fusion(bf16[8,128,2048]{2,1,0:T(8,128)(2,1)} %bitcast.98, s32[]{:T(128)S(6)} %select_n.61), kind=kLoop, calls=%fused_computation.115 | loop fusion | bytes 4194308 | tf_op jit(solution)/shard_map/dynamic_slice | solution.py:97
  10.4 7.3 %all-to-all-start = ((bf16[8,128,1024]{2,1,0:T(8,128)(2,1)}), bf16[8,128,1024]{2,1,0:T(8,128)(2,1)S(1)}, u32[]{:S(2)}, u32[]{:S(2)}) async-start(bf16[8,128,1024]{2,1,0:T(8,128)(2,1)} %constant_dynamic-slice_fusion.4), calls=%async_computation | async-start | bytes 4194304 | tf_op jit(solution)/shard_map/all_to_all | solution.py:98
  18.4 2.1 collective-permute-start
  20.5 61.0 %collective-permute-done = bf16[256,1024]{1,0:T(8,128)(2,1)S(1)} collective-permute-done((bf16[256,1024]{1,0:T(8,128)(2,1)S(1)}, bf16[256,1024]{1,0:T(8,128)(2,1)S(1)}, u32[]{:S(2)}, u32[]{:S(2)}) %collective-permute-start) | collective-permute-done | bytes 524320 | tf_op jit(solution)/shard_map/ppermute | solution.py:106
  81.5 22.7 %collective-permute-done.1 = bf16[256,1024]{1,0:T(8,128)(2,1)S(1)} collective-permute-done((bf16[256,1024]{1,0:T(8,128)(2,1)S(1)}, bf16[256,1024]{1,0:T(8,128)(2,1)S(1)}, u32[]{:S(2)}, u32[]{:S(2)}) %collective-permute-start.1) | collective-permute-done | bytes 524320 | tf_op jit(solution)/shard_map/ppermute | solution.py:106
  105.1 13.9 %collective-permute-done.2 = bf16[256,1024]{1,0:T(8,128)(2,1)} collective-permute-done((bf16[256,1024]{1,0:T(8,128)(2,1)S(1)}, bf16[256,1024]{1,0:T(8,128)(2,1)}, u32[]{:S(2)}, u32[]{:S(2)}) %collective-permute-start.2) | collective-permute-done | bytes 524320 | tf_op jit(solution)/shard_map/ppermute | solution.py:106
  119.0 5.6 %collective-permute-start.3 = (bf16[256,1024]{1,0:T(8,128)(2,1)}, bf16[256,1024]{1,0:T(8,128)(2,1)}, u32[]{:S(2)}, u32[]{:S(2)}) collective-permute-start(bf16[256,1024]{1,0:T(8,128)(2,1)} %collective-permute-done.2), channel_id=1, source_target_pairs={{0,2},{2,4},{4,6},{6,8},{8,10},{10,12},{12,14},{14,0},{1,3},{3,5},... | collective-permute-start | bytes 1572872 | tf_op jit(solution)/shard_map/ppermute | solution.py:106
  125.4 13.6 %all-to-all-start.1 = ((f32[8,16,128]{2,1,0:T(8,128)}), f32[8,16,128]{2,1,0:T(8,128)S(1)}, u32[]{:S(2)}, u32[]{:S(2)}) async-start(f32[8,16,128]{2,1,0:T(8,128)} %copy.36), calls=%async_computation.1 | async-start | bytes 131072 | tf_op jit(solution)/shard_map/all_to_all | solution.py:101
  141.1 2.1 collective-permute-start.4
  143.3 13.9 %collective-permute-done.4 = bf16[256,1024]{1,0:T(8,128)(2,1)S(1)} collective-permute-done((bf16[256,1024]{1,0:T(8,128)(2,1)}, bf16[256,1024]{1,0:T(8,128)(2,1)S(1)}, u32[]{:S(2)}, u32[]{:S(2)}) %collective-permute-start.4) | collective-permute-done | bytes 524320 | tf_op jit(solution)/shard_map/ppermute | solution.py:106
  157.3 14.8 %collective-permute-done.5 = bf16[256,1024]{1,0:T(8,128)(2,1)S(1)} collective-permute-done((bf16[256,1024]{1,0:T(8,128)(2,1)S(1)}, bf16[256,1024]{1,0:T(8,128)(2,1)S(1)}, u32[]{:S(2)}, u32[]{:S(2)}) %collective-permute-start.5) | collective-permute-done | bytes 524320 | tf_op jit(solution)/shard_map/ppermute | solution.py:106
  172.1 2.0 fusion.34
  174.3 11.8 %collective-permute-done.6 = bf16[256,1024]{1,0:T(8,128)(2,1)S(1)} collective-permute-done((bf16[256,1024]{1,0:T(8,128)(2,1)S(1)}, bf16[256,1024]{1,0:T(8,128)(2,1)S(1)}, u32[]{:S(2)}, u32[]{:S(2)}) %collective-permute-start.6) | collective-permute-done | bytes 524320 | tf_op jit(solution)/shard_map/ppermute | solution.py:106
  186.2 1.1 constant_dynamic-update-slice_fusion.12
  187.3 1.1 constant_dynamic-update-slice_fusion.11
  188.4 1.1 constant_dynamic-update-slice_fusion.10
  189.7 1.1 constant_dynamic-update-slice_fusion.4
  192.0 3.2 %copy-done.1 = bf16[4096,1024]{1,0:T(8,128)(2,1)} copy-done((bf16[4096,1024]{1,0:T(8,128)(2,1)}, bf16[4096,1024]{1,0:T(8,128)(2,1)S(1)}, u32[]{:S(2)}) %copy-start.1) | copy-done | bytes 8388632
  195.9 3.1 %fusion = f32[1024]{0:T(1024)S(1)} fusion(bf16[1024,2048]{1,0:T(8,128)(2,1)} %all-gather.5.cloned.1.call-done), kind=kLoop, calls=%fused_computation.2 | loop fusion | flops 6290432 | bytes 4198400 | tf_op jit(solution)/shard_map/reduce_sum | solution.py:12
  199.0 3.4 %fusion.16 = f32[16,1024]{1,0:T(8,128)S(1)} fusion(bf16[2048,8]{0,1:T(8,128)(2,1)S(1)} %get-tuple-element.19, bf16[2048,8]{0,1:T(8,128)(2,1)S(1)} %get-tuple-element.20, bf16[1024,2048]{1,0:T(8,128)(2,1)} %all-gather.5.cloned.1.call-done, f32[2048]{0:T(1024)S(1)} %convert_element_type.64, f32[1024]{0:T(1024)S(1)} %add_rsqrt_fusion), kind=kOutput, calls=%fused_computation.24 | convolution fusion | flops 75628544 | bytes 4337664 | tf_op jit(solution)/shard_map/dot_general | solution.py:17
  202.7 30.6 %all-gather = f32[64,8]{1,0:T(8,128)S(1)} all-gather(f32[8,8]{1,0:T(8,128)S(1)} %copy.38), channel_id=2, replica_groups=mesh['gr'=2,'sp'=8,'tp'=2] {'sp'}, dimensions={0}, use_global_device_ids=true | all-gather | bytes 2304 | tf_op jit(solution)/shard_map/all_gather | solution.py:30
  234.1 4.6 %multiply_convert_fusion = bf16[1024,512]{1,0:T(8,128)(2,1)S(1)} fusion(bf16[2048,512]{1,0:T(8,128)(2,1)S(1)} %copy-done.2, bf16[1024,2048]{1,0:T(8,128)(2,1)} %all-gather.5.cloned.1.call-done, f32[2048]{0:T(1024)S(1)} %convert_element_type.64, f32[1024]{0:T(1024)S(1)} %add_rsqrt_fusion), kind=kOutput, calls=%fused_computation.9 | convolution fusion | flops 2156920832 | bytes 7352320 | tf_op jit(solution)/shard_map/dot_general | solution.py:124
  239.3 8.0 %fusion.7 = bf16[1024,1024]{1,0:T(8,128)(2,1)S(1)} fusion(bf16[4096,1024]{1,0:T(8,128)(2,1)} %copy-done.1, s32[]{:T(128)S(6)} %select_n.63, bf16[1024,2048]{1,0:T(8,128)(2,1)} %all-gather.5.cloned.1.call-done, f32[2048]{0:T(1024)S(1)} %convert_element_type.64, f32[1024]{0:T(1024)S(1)} %add_rsqrt_fusion), kind=kOutput, calls=%fused_computation.10 | convolution fusion | flops 4304404480 | bytes 10498052 | tf_op jit(solution)/shard_map/dot_general | solution.py:125
  247.8 30.5 %all-gather.1 = f32[64,384]{1,0:T(8,128)S(1)} all-gather(f32[8,384]{1,0:T(8,128)S(1)} %pad_maximum_fusion.2), channel_id=3, replica_groups=mesh['gr'=2,'sp'=8,'tp'=2] {'sp'}, dimensions={0}, use_global_device_ids=true | all-gather | bytes 110592 | tf_op jit(solution)/shard_map/all_gather | solution.py:60
  (108 shorter events, 9.7 us)
Async XLA Ops:
  7.2 11.3 %copy-start.4 = (bf16[256,1024]{1,0:T(8,128)(2,1)S(1)}, bf16[256,1024]{1,0:T(8,128)(2,1)}, u32[]{:S(2)}) copy-start(bf16[256,1024]{1,0:T(8,128)(2,1)} %param.15) | copy-start | bytes 1572868
  7.2 117.4 %copy-start.9 = (f32[4,256,2,8]{1,3,2,0:T(8,128)S(1)}, f32[4,256,2,8]{1,3,2,0:T(8,128)}, u32[]{:S(2)}) copy-start(f32[4,256,2,8]{1,3,2,0:T(8,128)} %param.19) | copy-start | bytes 196612
  7.2 118.1 %copy-start.12 = (bf16[2048,16]{0,1:T(8,128)(2,1)S(1)}, bf16[2048,16]{0,1:T(8,128)(2,1)}, u32[]{:S(2)}) copy-start(bf16[2048,16]{0,1:T(8,128)(2,1)} %param.16) | copy-start | bytes 196612
  7.2 118.1 %copy-start.11 = (bf16[2048,16]{0,1:T(8,128)(2,1)S(1)}, bf16[2048,16]{0,1:T(8,128)(2,1)}, u32[]{:S(2)}) copy-start(bf16[2048,16]{0,1:T(8,128)(2,1)} %param.17) | copy-start | bytes 196612
  7.2 132.5 %copy-start.13 = (bf16[2048]{0:T(1024)(128)(2,1)S(1)}, bf16[2048]{0:T(1024)(128)(2,1)}, u32[]{:S(2)}) copy-start(bf16[2048]{0:T(1024)(128)(2,1)} %param.13) | copy-start | bytes 12292
  7.2 132.5 %copy-start.10 = (bf16[4,2048]{1,0:T(4,128)(2,1)S(1)}, bf16[4,2048]{1,0:T(4,128)(2,1)}, u32[]{:S(2)}) copy-start(bf16[4,2048]{1,0:T(4,128)(2,1)} %param.11) | copy-start | bytes 49156
  7.2 133.9 %copy-start.14 = (bf16[4,512]{1,0:T(4,128)(2,1)S(1)}, bf16[4,512]{1,0:T(4,128)(2,1)}, u32[]{:S(2)}) copy-start(bf16[4,512]{1,0:T(4,128)(2,1)} %param.12) | copy-start | bytes 12292
  10.4 115.0 %all-to-all-start = ((bf16[8,128,1024]{2,1,0:T(8,128)(2,1)}), bf16[8,128,1024]{2,1,0:T(8,128)(2,1)S(1)}, u32[]{:S(2)}, u32[]{:S(2)}) async-start(bf16[8,128,1024]{2,1,0:T(8,128)(2,1)} %constant_dynamic-slice_fusion.4), calls=%async_computation | async-start | bytes 4194304 | tf_op jit(solution)/shard_map/all_to_all | solution.py:98
  17.7 154.4 %all-gather.7.cloned.1.call-start = ((), (), s32[]{:S(2)}) async-start(), calls=%async_computation.3 | async-start | bytes 2359296 | tf_op jit(solution)/shard_map/all_gather | solution.py:103
  18.4 63.1 %collective-permute-start = (bf16[256,1024]{1,0:T(8,128)(2,1)S(1)}, bf16[256,1024]{1,0:T(8,128)(2,1)S(1)}, u32[]{:S(2)}, u32[]{:S(2)}) collective-permute-start(bf16[256,1024]{1,0:T(8,128)(2,1)S(1)} %copy-done.4), channel_id=1, source_target_pairs={{0,2},{2,4},{4,6},{6,8},{8,10},{10,12},{12,14},{14,0},{1,3},{3,5},... | collective-permute-start | bytes 1572872 | tf_op jit(solution)/shard_map/ppermute | solution.py:106
  81.5 22.7 %collective-permute-start.1 = (bf16[256,1024]{1,0:T(8,128)(2,1)S(1)}, bf16[256,1024]{1,0:T(8,128)(2,1)S(1)}, u32[]{:S(2)}, u32[]{:S(2)}) collective-permute-start(bf16[256,1024]{1,0:T(8,128)(2,1)S(1)} %collective-permute-done), channel_id=1, source_target_pairs={{0,2},{2,4},{4,6},{6,8},{8,10},{10,12},{12,14},{14,0},{1,3},{3,5},... | collective-permute-start | bytes 1572872 | tf_op jit(solution)/shard_map/ppermute | solution.py:106
  105.0 13.9 %collective-permute-start.2 = (bf16[256,1024]{1,0:T(8,128)(2,1)S(1)}, bf16[256,1024]{1,0:T(8,128)(2,1)}, u32[]{:S(2)}, u32[]{:S(2)}) collective-permute-start(bf16[256,1024]{1,0:T(8,128)(2,1)S(1)} %collective-permute-done.1), channel_id=1, source_target_pairs={{0,2},{2,4},{4,6},{6,8},{8,10},{10,12},{12,14},{14,0},{1,3},{3,5},... | collective-permute-start | bytes 1572872 | tf_op jit(solution)/shard_map/ppermute | solution.py:106
  119.0 22.1 %collective-permute-start.3 = (bf16[256,1024]{1,0:T(8,128)(2,1)}, bf16[256,1024]{1,0:T(8,128)(2,1)}, u32[]{:S(2)}, u32[]{:S(2)}) collective-permute-start(bf16[256,1024]{1,0:T(8,128)(2,1)} %collective-permute-done.2), channel_id=1, source_target_pairs={{0,2},{2,4},{4,6},{6,8},{8,10},{10,12},{12,14},{14,0},{1,3},{3,5},... | collective-permute-start | bytes 1572872 | tf_op jit(solution)/shard_map/ppermute | solution.py:106
  125.4 13.6 %copy-start = (bf16[8,128,1024]{2,1,0:T(8,128)(2,1)}, bf16[8,128,1024]{2,1,0:T(8,128)(2,1)S(1)}, u32[]{:S(2)}) copy-start(bf16[8,128,1024]{2,1,0:T(8,128)(2,1)S(1)} %all-to-all-done) | copy-start | bytes 6291460
  125.4 77.1 %all-to-all-start.1 = ((f32[8,16,128]{2,1,0:T(8,128)}), f32[8,16,128]{2,1,0:T(8,128)S(1)}, u32[]{:S(2)}, u32[]{:S(2)}) async-start(f32[8,16,128]{2,1,0:T(8,128)} %copy.36), calls=%async_computation.1 | async-start | bytes 131072 | tf_op jit(solution)/shard_map/all_to_all | solution.py:101
  138.9 57.0 %all-gather.5.cloned.1.call-start = ((), (), s32[]{:S(2)}) async-start(), calls=%async_computation.2 | async-start | bytes 6291456 | tf_op jit(solution)/shard_map/all_gather | solution.py:99
  139.7 52.2 %copy-start.6 = (bf16[256,1024]{1,0:T(8,128)(2,1)S(1)}, bf16[256,1024]{1,0:T(8,128)(2,1)}, u32[]{:S(2)}) copy-start(bf16[256,1024]{1,0:T(8,128)(2,1)} %copy-done.5) | copy-start | bytes 1572868
  141.1 16.0 %collective-permute-start.4 = (bf16[256,1024]{1,0:T(8,128)(2,1)}, bf16[256,1024]{1,0:T(8,128)(2,1)S(1)}, u32[]{:S(2)}, u32[]{:S(2)}) collective-permute-start(bf16[256,1024]{1,0:T(8,128)(2,1)} %collective-permute-done.3), channel_id=1, source_target_pairs={{0,2},{2,4},{4,6},{6,8},{8,10},{10,12},{12,14},{14,0},{1,3},{3,5},... | collective-permute-start | bytes 1572872 | tf_op jit(solution)/shard_map/ppermute | solution.py:106
  157.2 14.9 %collective-permute-start.5 = (bf16[256,1024]{1,0:T(8,128)(2,1)S(1)}, bf16[256,1024]{1,0:T(8,128)(2,1)S(1)}, u32[]{:S(2)}, u32[]{:S(2)}) collective-permute-start(bf16[256,1024]{1,0:T(8,128)(2,1)S(1)} %collective-permute-done.4), channel_id=1, source_target_pairs={{0,2},{2,4},{4,6},{6,8},{8,10},{10,12},{12,14},{14,0},{1,3},{3,5},... | collective-permute-start | bytes 1572872 | tf_op jit(solution)/shard_map/ppermute | solution.py:106
  172.1 14.0 %collective-permute-start.6 = (bf16[256,1024]{1,0:T(8,128)(2,1)S(1)}, bf16[256,1024]{1,0:T(8,128)(2,1)S(1)}, u32[]{:S(2)}, u32[]{:S(2)}) collective-permute-start(bf16[256,1024]{1,0:T(8,128)(2,1)S(1)} %collective-permute-done.5), channel_id=1, source_target_pairs={{0,2},{2,4},{4,6},{6,8},{8,10},{10,12},{12,14},{14,0},{1,3},{3,5},... | collective-permute-start | bytes 1572872 | tf_op jit(solution)/shard_map/ppermute | solution.py:106
  195.2 7.2 %copy-start.15 = (f32[8]{0:T(128)S(1)}, f32[8]{0:T(128)}, u32[]{:S(2)}) copy-start(f32[8]{0:T(128)} %param.18) | copy-start | bytes 100
  195.2 38.8 %copy-start.2 = (bf16[2048,512]{1,0:T(8,128)(2,1)S(1)}, bf16[2048,512]{1,0:T(8,128)(2,1)}, u32[]{:S(2)}) copy-start(bf16[2048,512]{1,0:T(8,128)(2,1)} %all-gather.7.cloned.1.call-done) | copy-start | bytes 6291460
  238.7 8.7 %copy-start.7 = (bf16[1024,512]{1,0:T(8,128)(2,1)}, bf16[1024,512]{1,0:T(8,128)(2,1)S(1)}, u32[]{:S(2)}) copy-start(bf16[1024,512]{1,0:T(8,128)(2,1)S(1)} %multiply_convert_fusion) | copy-start | bytes 3145732
  247.4 32.4 %copy-start.3 = (bf16[1024,1024]{1,0:T(8,128)(2,1)}, bf16[1024,1024]{1,0:T(8,128)(2,1)S(1)}, u32[]{:S(2)}) copy-start(bf16[1024,1024]{1,0:T(8,128)(2,1)S(1)} %fusion.7) | copy-start | bytes 6291460
  (3 other events, 9.1 us)
Sparse Core Ops, SparseCore 0:
  20.6 85.1 all-gather.6
  141.9 15.0 all-gather.4
